TPU v7x, 32 devices: a whole 2x2x4 slice. The times are simulated.
32 devices in a mesh: sp: 8 (over z, y), tp: 4 (over x, core).
Axes of the slice: x: 2, y: 2, z: 4, core: 2. Of those that a mesh axis runs over, the one named last changes fastest.
Arguments:
- resid: bfloat16 [2048, 2048], P(('sp', 'tp')), may hold values from -6 to 6
- query_a: bfloat16 [2048, 4, 128], P('sp', 'tp')
- key_a: bfloat16 [2048, 4, 128], P('sp', 'tp')
- value_a: bfloat16 [2048, 4, 128], P('sp', 'tp'), may hold values from -6 to 6
- query_b: bfloat16 [2048, 4, 256], P('sp', 'tp')
- key_b: bfloat16 [2048, 4, 256], P('sp', 'tp')
- value_b: bfloat16 [2048, 4, 128], P('sp', 'tp'), may hold values from -6 to 6
- lambda_a: float32 [4], P('tp'), may hold values from 0.3 to 0.8
- lambda_b: float32 [4], P('tp'), may hold values from 0.3 to 0.8
- head_gain: float32 [128], replicated, may hold values from 0.1 to 1.9
- out_weight: bfloat16 [1024, 2048], replicated, may hold values from -0.1875 to 0.1875
- norm_gain: float32 [2048], replicated, may hold values from 0.1 to 1.9
- expert_ids: int32 [2048, 4], P(('sp', 'tp')), may hold values from 0 to 31, all different within a row; in each aligned block of 64 rows (0 to 63, 64 to 127, ...) at most 16 rows name the same one
- expert_mix: float32 [2048, 4], P(('sp', 'tp')), may hold values from 0.2 to 1
- gate_experts: bfloat16 [32, 2048, 1024], P(('sp', 'tp')), may hold values from -0.125 to 0.125
- up_experts: bfloat16 [32, 2048, 1024], P(('sp', 'tp')), may hold values from -0.125 to 0.125
- down_experts: bfloat16 [32, 1024, 2048], P(('sp', 'tp')), may hold values from -0.1875 to 0.1875
- shared_gate: bfloat16 [2048, 512], replicated, may hold values from -0.125 to 0.125
- shared_up: bfloat16 [2048, 512], replicated, may hold values from -0.125 to 0.125
- shared_down: bfloat16 [512, 2048], replicated, may hold values from -0.25 to 0.25
Outputs:
- layer_out: bfloat16 [2048, 2048], P(('sp', 'tp'))
Inputs may be any that keep to these rules, and one draw needn't show every extreme that they name: `expert_ids`: in each aligned block of 64 rows (the rows of one device) no expert is named more than 16 times, a bound that some block reaches.
All inputs are finite; a program needn't handle non-finite values.
Results may differ from a plain program's by a relative error of at most 0.017.
Values may be sent and summed in bfloat16 or wider, within the bound.
No kernel may reach another device: no remote copies, remote signals or barrier semaphores. Data moves between devices by JAX's collectives and lax.ppermute only.
A program may use at most 128 MiB of HBM per device.

v0:
```python
import math
import jax
import jax.numpy as jnp
from jax import lax
from jax.sharding import PartitionSpec as P

NEG_FILL = -1e30
EPSILON = 1e-05
HEAD_SCALE = 0.8
KEY_SPAN = 2048


def swiglu_rows(row_set, w_gate, w_up, w_down):
    gate_val = jnp.dot(row_set, w_gate, preferred_element_type=jnp.float32)
    up_val = jnp.dot(row_set, w_up, preferred_element_type=jnp.float32)
    hidden = (jax.nn.silu(gate_val) * up_val).astype(jnp.bfloat16)
    return jnp.dot(hidden, w_down, preferred_element_type=jnp.float32)


def online_update(state, query_map, key_map, value_block, causal, scaling):
    row_top, denoms, numerator = state
    scores = (
        jnp.einsum("qhd,khd->hqk", query_map, key_map, preferred_element_type=jnp.float32) * scaling
    )
    scores = jnp.where(causal, scores, NEG_FILL)
    new_top = jnp.maximum(row_top, jnp.max(scores, axis=2))
    exponent = jnp.where(causal, jnp.exp(scores - new_top[:, :, None]), 0.0)
    shrink = jnp.exp(row_top - new_top)
    denoms = denoms * shrink + jnp.sum(exponent, axis=2)
    numerator = numerator * jnp.transpose(shrink)[:, :, None] + jnp.einsum(
        "hqk,khe->qhe",
        exponent.astype(jnp.bfloat16),
        value_block,
        preferred_element_type=jnp.float32,
    )
    return (new_top, denoms, numerator)


def group_update(states, queries, key_block, value_block, causal):
    map_width = queries.shape[2] // 2
    scaling = map_width ** (-0.5)
    first_state = online_update(
        states[0],
        queries[:, :, :map_width],
        key_block[:, :, :map_width],
        value_block,
        causal,
        scaling,
    )
    second_state = online_update(
        states[1],
        queries[:, :, map_width:],
        key_block[:, :, map_width:],
        value_block,
        causal,
        scaling,
    )
    return (first_state, second_state)


def empty_state(query_rows, head_count, value_width):
    single = (
        jnp.full((head_count, query_rows), NEG_FILL, jnp.float32),
        jnp.zeros((head_count, query_rows), jnp.float32),
        jnp.zeros((query_rows, head_count, value_width), jnp.float32),
    )
    return (single, single)


def finish_group(states, lambdas, head_gain):
    first_out = states[0][2] / jnp.transpose(states[0][1])[:, :, None]
    second_out = states[1][2] / jnp.transpose(states[1][1])[:, :, None]
    differ = first_out - lambdas[None, :, None] * second_out
    scale_rms = lax.rsqrt(jnp.mean(differ * differ, axis=2, keepdims=True) + EPSILON)
    return (differ * scale_rms * head_gain[None, None, :] * HEAD_SCALE).astype(jnp.bfloat16)


def per_device(
    resid,
    query_a,
    key_a,
    value_a,
    query_b,
    key_b,
    value_b,
    lambda_a,
    lambda_b,
    head_gain,
    out_weight,
    norm_gain,
    expert_ids,
    expert_mix,
    gate_experts,
    up_experts,
    down_experts,
    shared_gate,
    shared_up,
    shared_down,
):
    query_rows = query_a.shape[0]
    value_width = value_a.shape[2]
    query_pos = lax.axis_index("sp") * query_rows + jnp.arange(query_rows, dtype=jnp.int32)
    start_state = (
        empty_state(query_rows, query_a.shape[1], value_width),
        empty_state(query_rows, query_b.shape[1], value_width),
    )
    key_piece_a = lax.all_gather(key_a, "sp", axis=0, tiled=True)
    value_piece_a = lax.all_gather(value_a, "sp", axis=0, tiled=True)
    key_piece_b = lax.all_gather(key_b, "sp", axis=0, tiled=True)
    value_piece_b = lax.all_gather(value_b, "sp", axis=0, tiled=True)
    piece_rows = key_piece_a.shape[0]
    step_rows = math.gcd(piece_rows, KEY_SPAN)

    def one_step(step_index, inner_state):
        begin_row = step_index * step_rows
        key_pos = begin_row + jnp.arange(step_rows, dtype=jnp.int32)
        causal = (key_pos[None, :] <= query_pos[:, None])[None]
        part_a = group_update(
            inner_state[0],
            query_a,
            lax.dynamic_slice_in_dim(key_piece_a, begin_row, step_rows, 0),
            lax.dynamic_slice_in_dim(value_piece_a, begin_row, step_rows, 0),
            causal,
        )
        part_b = group_update(
            inner_state[1],
            query_b,
            lax.dynamic_slice_in_dim(key_piece_b, begin_row, step_rows, 0),
            lax.dynamic_slice_in_dim(value_piece_b, begin_row, step_rows, 0),
            causal,
        )
        return (part_a, part_b)

    state_a, state_b = lax.fori_loop(0, piece_rows // step_rows, one_step, start_state)
    heads_a = finish_group(state_a, lambda_a, head_gain)
    heads_b = finish_group(state_b, lambda_b, head_gain)
    tok_dev = resid.shape[0]
    back_a, back_b = (
        lax.all_to_all(heads_a, "tp", split_axis=0, concat_axis=1, tiled=True),
        lax.all_to_all(heads_b, "tp", split_axis=0, concat_axis=1, tiled=True),
    )
    joined = jnp.concatenate([back_a.reshape(tok_dev, -1), back_b.reshape(tok_dev, -1)], axis=1)
    project = jnp.dot(joined, out_weight, preferred_element_type=jnp.float32)
    middle = (resid.astype(jnp.float32) + project).astype(jnp.bfloat16)
    middle_f = middle.astype(jnp.float32)
    normed = (
        middle_f
        * lax.rsqrt(jnp.mean(middle_f * middle_f, axis=1, keepdims=True) + EPSILON)
        * norm_gain[None, :]
    ).astype(jnp.bfloat16)
    shared = swiglu_rows(normed, shared_gate, shared_up, shared_down)
    top_count = expert_ids.shape[1]
    model_width = normed.shape[1]
    sp_count = lax.axis_size("sp")
    tp_count = lax.axis_size("tp")
    expert_total = sp_count * tp_count
    pair_count = tok_dev * top_count
    capacity = max(2, 2 * pair_count // expert_total)
    flat_ids = expert_ids.reshape(-1)
    one_hot = (flat_ids[:, None] == jnp.arange(expert_total, dtype=jnp.int32)[None, :]).astype(
        jnp.int32
    )
    pair_rank = jnp.sum((jnp.cumsum(one_hot, axis=0) - one_hot) * one_hot, axis=1)
    pair_token = jnp.arange(pair_count, dtype=jnp.int32) // top_count
    send_rows = (
        jnp.zeros((expert_total, capacity, model_width), jnp.bfloat16)
        .at[flat_ids, pair_rank]
        .set(normed[pair_token])
    )
    arrived = lax.all_to_all(send_rows, ("sp", "tp"), split_axis=0, concat_axis=0, tiled=True)
    arrived_shape = arrived.shape
    flat_rows = arrived.reshape(-1, arrived_shape[-1])
    result = swiglu_rows(flat_rows, gate_experts[0], up_experts[0], down_experts[0]).astype(
        jnp.bfloat16
    )
    finished = result.reshape(arrived_shape)
    returned = lax.all_to_all(finished, ("sp", "tp"), split_axis=0, concat_axis=0, tiled=True)
    chosen = returned[flat_ids, pair_rank].reshape(tok_dev, top_count, model_width)
    routed = jnp.sum(chosen.astype(jnp.float32) * expert_mix[:, :, None], axis=1)
    return (middle_f + shared + routed).astype(jnp.bfloat16)


def solution(mesh):
    in_specs = (
        P(("sp", "tp"), None),
        P("sp", "tp", None),
        P("sp", "tp", None),
        P("sp", "tp", None),
        P("sp", "tp", None),
        P("sp", "tp", None),
        P("sp", "tp", None),
        P("tp"),
        P("tp"),
        P(),
        P(),
        P(),
        P(("sp", "tp"), None),
        P(("sp", "tp"), None),
        P(("sp", "tp"), None, None),
        P(("sp", "tp"), None, None),
        P(("sp", "tp"), None, None),
        P(),
        P(),
        P(),
    )
    out_specs = P(("sp", "tp"), None)
    return jax.shard_map(
        per_device, mesh=mesh, in_specs=in_specs, out_specs=out_specs, check_vma=False
    )
```

profile of v0, /device:TPU:0, one launch (start us, length us, event | category | flops | bytes accessed | tf_op | source)
XLA Modules:
  0.0 333.9 jit_solution(18437636033774966400)
XLA Ops:
  6.5 0.7 all-gather.2.cloned.1.call-update
  7.3 33.6 %all_gather.12 = bf16[2048,1,128]{2,0,1:T(8,128)(2,1)S(1)} all-gather(bf16[256,1,128]{2,0,1:T(8,128)(2,1)} %param.22), channel_id=1, replica_groups=mesh['sp'=8,'tp'=4] {'sp'}, dimensions={0}, use_global_device_ids=true | all-gather | bytes 589824 | tf_op jit(solution)/shard_map/all_gather | solution.py:107
  40.9 0.8 copy.35
  41.6 0.1 eq.29
  41.8 0.6 reduce-window.6
  42.4 0.2 slice_reduce_fusion
  42.6 0.1 eq.25
  42.7 0.1 reshape.406
  44.1 0.1 fusion.73
  44.2 2.8 fusion.88
  47.0 1.8 fusion.89
  48.9 31.4 %all_gather.15 = bf16[2048,1,128]{2,0,1:T(8,128)(2,1)S(1)} all-gather(bf16[256,1,128]{2,0,1:T(8,128)(2,1)S(1)} %copy-done.5), channel_id=1, replica_groups=mesh['sp'=8,'tp'=4] {'sp'}, dimensions={0}, use_global_device_ids=true | all-gather | bytes 589824 | tf_op jit(solution)/shard_map/all_gather | solution.py:110
  80.3 31.5 %all_gather.13 = bf16[2048,1,128]{2,0,1:T(8,128)(2,1)S(1)} all-gather(bf16[256,1,128]{2,0,1:T(8,128)(2,1)S(1)} %copy-done.6), channel_id=1, replica_groups=mesh['sp'=8,'tp'=4] {'sp'}, dimensions={0}, use_global_device_ids=true | all-gather | bytes 589824 | tf_op jit(solution)/shard_map/all_gather | solution.py:108
  111.8 1.8 fusion.91
  113.6 1.8 fusion.90
  115.4 2.1 fusion.19
  117.5 0.7 fusion.38
  118.2 0.7 multiply_reduce_fusion.2
  118.9 0.7 fusion.32
  119.6 0.7 multiply_reduce_fusion.3
  120.4 0.6 broadcast.531
  121.0 0.7 reduce.22
  121.7 0.1 copy.50
  121.8 0.7 reshape.432
  122.5 3.3 all-to-all-start.1
  125.8 0.7 reduce.23
  126.5 0.1 copy.51
  126.6 0.6 reshape.434
  127.3 2.6 all-to-all-done.1
  129.9 3.3 all-to-all-start
  133.3 3.9 %all-to-all-done = bf16[4,2,4096]{2,1,0:T(2,128)(2,1)S(1)} async-done(((bf16[4,2,4096]{2,1,0:T(2,128)(2,1)}), bf16[4,2,4096]{2,1,0:T(2,128)(2,1)S(1)}, u32[]{:S(2)}, u32[]{:S(2)}) %all-to-all-start) | async-done | bytes 65568 | tf_op jit(solution)/shard_map/all_to_all | solution.py:139
  137.4 3.2 multiply_reduce_fusion.1
  140.6 0.1 multiply_convert_fusion.1
  140.7 2.3 gather_fusion
  143.1 1.6 broadcast_in_dim.49
  144.7 46.2 %scatter_fusion = bf16[32,16,2048]{2,1,0:T(8,128)(2,1)} fusion(bf16[32,16,2048]{2,1,0:T(8,128)(2,1)} %broadcast_in_dim.49, s32[256]{0:T(256)S(1)} %bitcast.169, bf16[256,2048]{1,0:T(8,128)(2,1)} %gather_fusion), kind=kCustom, calls=%fused_computation.2 | custom fusion | bytes 3147776 | tf_op jit(solution)/shard_map/scatter | solution.py:168
  190.9 53.7 %all_to_all.40 = bf16[32,16,2048]{2,1,0:T(8,128)(2,1)S(1)} all-to-all(bf16[32,16,2048]{2,1,0:T(8,128)(2,1)} %scatter_fusion), channel_id=1, replica_groups=mesh['sp'=8,'tp'=4] {'sp','tp'}, dimensions={0} | all-to-all | bytes 4194304 | tf_op jit(solution)/shard_map/all_to_all | solution.py:170
  244.6 1.3 copy-done.3
  246.0 3.6 %fusion.4 = f32[512,1024]{1,0:T(8,128)} fusion(bf16[512,2048]{1,0:T(8,128)(2,1)S(1)} %bitcast.171, bf16[1,2048,1024]{2,1,0:T(8,128)(2,1)S(1)} %copy-done.10), kind=kOutput, calls=%fused_computation.7 | convolution fusion | flops 2147483648 | bytes 8388608 | tf_op jit(solution)/shard_map/dot_general | solution.py:14
  249.6 10.6 %fusion.6 = bf16[512,2048]{1,0:T(8,128)(2,1)} fusion(bf16[1,1024,2048]{2,1,0:T(8,128)(2,1)} %param.36, f32[512,1024]{1,0:T(8,128)} %fusion.4, bf16[512,2048]{1,0:T(8,128)(2,1)} %bitcast.172, bf16[1,2048,1024]{2,1,0:T(8,128)(2,1)} %param.35), kind=kOutput, calls=%fused_computation.9 | convolution fusion | flops 4299161600 | bytes 14680064 | tf_op jit(solution)/shard_map/dot_general | solution.py:17
  260.2 3.8 %all-to-all-start.3 = ((bf16[32,16,2048]{2,1,0:T(8,128)(2,1)}), bf16[32,16,2048]{2,1,0:T(8,128)(2,1)}, u32[]{:S(2)}, u32[]{:S(2)}) async-start(bf16[32,16,2048]{2,1,0:T(8,128)(2,1)} %bitcast.170), calls=%async_computation.3 | async-start | bytes 4194304 | tf_op jit(solution)/shard_map/all_to_all | solution.py:177
  264.0 0.7 copy.39
  264.7 2.1 fusion.92
  266.8 45.9 %all-to-all-done.3 = bf16[32,16,2048]{2,1,0:T(8,128)(2,1)} async-done(((bf16[32,16,2048]{2,1,0:T(8,128)(2,1)}), bf16[32,16,2048]{2,1,0:T(8,128)(2,1)}, u32[]{:S(2)}, u32[]{:S(2)}) %all-to-all-start.3) | async-done | bytes 2097184 | tf_op jit(solution)/shard_map/all_to_all | solution.py:177
  312.7 5.1 %gather_fusion.1 = bf16[256,2048]{1,0:T(8,128)(2,1)} fusion(bf16[32,16,2048]{2,1,0:T(8,128)(2,1)} %all-to-all-done.3, s32[256]{0:T(256)S(1)} %bitcast.168), kind=kCustom, calls=%fused_computation.1 | custom fusion | bytes 2099200 | tf_op jit(solution)/shard_map/gather | solution.py:178
  317.9 2.7 reshape.410
  320.6 3.2 multiply_reduce_fusion
  323.8 3.2 fusion.14
  (52 shorter events, 0.6 us)
Async XLA Ops:
  6.5 317.3 %copy-start = (bf16[512,2048]{1,0:T(8,128)(2,1)S(1)}, bf16[512,2048]{1,0:T(8,128)(2,1)}, u32[]{:S(2)}) copy-start(bf16[512,2048]{1,0:T(8,128)(2,1)} %param.39) | copy-start | bytes 6291460
  6.5 40.5 %copy-start.12 = (bf16[256,1,128]{2,0,1:T(8,128)(2,1)S(1)}, bf16[256,1,128]{2,0,1:T(8,128)(2,1)}, u32[]{:S(2)}) copy-start(bf16[256,1,128]{2,0,1:T(8,128)(2,1)} %param.21) | copy-start | bytes 196612
  6.5 105.2 %all-gather.2.cloned.1.call-start = ((), (), s32[]{:S(2)}) async-start(), calls=%async_computation.4 | async-start | bytes 1179648 | tf_op jit(solution)/shard_map/all_gather | solution.py:109
  47.0 1.9 copy-start.5
  47.0 33.3 %copy-start.6 = (bf16[256,1,128]{2,0,1:T(8,128)(2,1)S(1)}, bf16[256,1,128]{2,0,1:T(8,128)(2,1)}, u32[]{:S(2)}) copy-start(bf16[256,1,128]{2,0,1:T(8,128)(2,1)} %param.23) | copy-start | bytes 196612
  47.0 64.8 %copy-start.11 = (bf16[256,1,256]{2,0,1:T(8,128)(2,1)S(1)}, bf16[256,1,256]{2,0,1:T(8,128)(2,1)}, u32[]{:S(2)}) copy-start(bf16[256,1,256]{2,0,1:T(8,128)(2,1)} %param.24) | copy-start | bytes 393220
  111.8 3.6 %copy-start.2 = (f32[256,2048]{1,0:T(8,128)S(1)}, f32[256,2048]{1,0:T(8,128)}, u32[]{:S(2)}) copy-start(f32[256,2048]{1,0:T(8,128)} %get-tuple-element.62) | copy-start | bytes 6291460
  113.6 1.8 copy-start.1
  119.6 0.7 copy-start.9
  120.3 17.1 %copy-start.4 = (bf16[64,2048]{1,0:T(8,128)(2,1)S(1)}, bf16[64,2048]{1,0:T(8,128)(2,1)}, u32[]{:S(2)}) copy-start(bf16[64,2048]{1,0:T(8,128)(2,1)} %param.20) | copy-start | bytes 786436
  122.5 7.4 %all-to-all-start.1 = ((bf16[4,2,4096]{2,1,0:T(2,128)(2,1)}), bf16[4,2,4096]{2,1,0:T(2,128)(2,1)S(1)}, u32[]{:S(2)}, u32[]{:S(2)}) async-start(bf16[4,2,4096]{2,1,0:T(2,128)(2,1)} %reshape.432), calls=%async_computation.1 | async-start | bytes 131072 | tf_op jit(solution)/shard_map/all_to_all | solution.py:140
  129.9 7.4 %all-to-all-start = ((bf16[4,2,4096]{2,1,0:T(2,128)(2,1)}), bf16[4,2,4096]{2,1,0:T(2,128)(2,1)S(1)}, u32[]{:S(2)}, u32[]{:S(2)}) async-start(bf16[4,2,4096]{2,1,0:T(2,128)(2,1)} %reshape.434), calls=%async_computation | async-start | bytes 131072 | tf_op jit(solution)/shard_map/all_to_all | solution.py:139
  137.4 3.2 copy-start.7
  190.9 55.0 %copy-start.10 = (bf16[1,2048,1024]{2,1,0:T(8,128)(2,1)S(1)}, bf16[1,2048,1024]{2,1,0:T(8,128)(2,1)}, u32[]{:S(2)}) copy-start(bf16[1,2048,1024]{2,1,0:T(8,128)(2,1)} %param.34) | copy-start | bytes 12582916
  244.6 1.3 copy-start.3
  260.2 3.8 %copy-start.8 = (f32[64,4]{0,1:T(4,128)S(1)}, f32[64,4]{0,1:T(4,128)}, u32[]{:S(2)}) copy-start(f32[64,4]{0,1:T(4,128)} %param.33) | copy-start | bytes 3076
  260.2 52.5 %all-to-all-start.3 = ((bf16[32,16,2048]{2,1,0:T(8,128)(2,1)}), bf16[32,16,2048]{2,1,0:T(8,128)(2,1)}, u32[]{:S(2)}, u32[]{:S(2)}) async-start(bf16[32,16,2048]{2,1,0:T(8,128)(2,1)} %bitcast.170), calls=%async_computation.3 | async-start | bytes 4194304 | tf_op jit(solution)/shard_map/all_to_all | solution.py:177
Sparse Core Ops, SparseCore 0:
  9.5 43.6 all-gather.1
where the time goes:
time: 336 us; the launch traced here: 334 us
  blocking collectives  150 us (45%)
  local copies, waits for them, and re-layouts  63.9 us (19%)
  waiting for transfers between devices  53.1 us (16%)
  matrix products  33.6 us (10%)
  between operations  15.1 us (4%)
  starting transfers between devices  10.4 us (3%)
  other arithmetic  7.7 us (2%)
    all_to_all x1, blocking collectives, per_device(): lax.all_to_all(send_rows, ('sp', 'tp'), split_axis=0, concat_axis=0, tile...  53.7 us
    scatter x1, local copies, waits for them, and re-layouts, per_device(): send_rows = jnp.zeros((expert_total, capacity, model_width), jnp.bfloat16...  46.2 us
    all_to_all x1, waiting for transfers between devices, per_device(): lax.all_to_all(finished, ('sp', 'tp'), split_axis=0, concat_axis=0, tiled...  45.9 us
    all_gather x1, blocking collectives, per_device(): key_piece_a = lax.all_gather(key_a, 'sp', axis=0, tiled=True)  33.6 us
    all_gather x1, blocking collectives, per_device(): value_piece_a = lax.all_gather(value_a, 'sp', axis=0, tiled=True)  31.5 us
    all_gather x1, blocking collectives, per_device(): value_piece_b = lax.all_gather(value_b, 'sp', axis=0, tiled=True)  31.4 us
    dot_general x2, matrix products, swiglu_rows(): return jnp.dot(hidden, w_down, preferred_element_type=jnp.float32)  13.8 us
    dot_general x4, matrix products, online_update(): jnp.einsum('qhd,khd->hqk', query_map, key_map, preferred_element_type=jnp...  8.17 us
  transfers between devices with their start and end apart: 4, of which 3 were waited for; matrix products, arithmetic and copies ran while one was open for 3% of the time, Pallas kernels for 0%

commit v1 on v0

--- a/solution.py
+++ b/solution.py
@@ -8,6 +8,22 @@
 EPSILON = 1e-05
 HEAD_SCALE = 0.8
 KEY_SPAN = 2048
+
+
+def gather_around(x, axis, dim):
+    ways, here, lap = (lax.axis_size(axis), lax.axis_index(axis), x.shape[dim])
+    shape = [n * ways if d == dim else n for d, n in enumerate(x.shape)]
+    full = lax.dynamic_update_slice_in_dim(jnp.zeros(shape, x.dtype), x, here * lap, axis=dim)
+    going_up = going_down = x
+    for far in range(1, ways // 2 + 1):
+        going_up = lax.ppermute(going_up, axis, [(d, (d + 1) % ways) for d in range(ways)])
+        full = lax.dynamic_update_slice_in_dim(full, going_up, (here - far) % ways * lap, axis=dim)
+        if 2 * far < ways:
+            going_down = lax.ppermute(going_down, axis, [(d, (d - 1) % ways) for d in range(ways)])
+            full = lax.dynamic_update_slice_in_dim(
+                full, going_down, (here + far) % ways * lap, axis=dim
+            )
+    return full
 
 
 def swiglu_rows(row_set, w_gate, w_up, w_down):
@@ -104,7 +120,7 @@
         empty_state(query_rows, query_a.shape[1], value_width),
         empty_state(query_rows, query_b.shape[1], value_width),
     )
-    key_piece_a = lax.all_gather(key_a, "sp", axis=0, tiled=True)
+    key_piece_a = gather_around(key_a, "sp", 0)
     value_piece_a = lax.all_gather(value_a, "sp", axis=0, tiled=True)
     key_piece_b = lax.all_gather(key_b, "sp", axis=0, tiled=True)
     value_piece_b = lax.all_gather(value_b, "sp", axis=0, tiled=True)

time: 336 us -> 331 us (0.985)
  blocking collectives: 150 us -> 117 us
  starting transfers between devices: 10.4 us -> 25.9 us
  waiting for transfers between devices: 53.1 us -> 60.2 us
  local copies, waits for them, and re-layouts: 63.9 us -> 69.7 us
    all_gather x1 -> x0, blocking collectives: 33.6 us -> none  [per_device(): key_piece_a = lax.all_gather(key_a, 'sp', axis=0, tiled=True)]
    ppermute x0 -> x7, starting transfers between devices: none -> 15.6 us  [the longest x3 12.5 us: gather_around(): lax.ppermute(going_down, axis, [(d, (d - 1) % ways) for d in range(ways)])]
    ppermute x0 -> x7, waiting for transfers between devices: none -> 7.71 us  [the longest x4 7.71 us: gather_around(): lax.ppermute(going_up, axis, [(d, (d + 1) % ways) for d in range(ways)])]
    dynamic_update_slice x0 -> x8, local copies, waits for them, and re-layouts: none -> 4.98 us  [the longest x4 2.5 us: gather_around(): lax.dynamic_update_slice_in_dim(full, going_up, (here - far) % ways * lap...]
  transfers between devices with their start and end apart: 4 -> 11, of which waited for: 3 -> 6; matrix products, arithmetic and copies ran while one was open for 3% -> 6% of each run, Pallas kernels for 0% -> 0%
where the time goes in v1:
time: 331 us; the launch traced here: 329 us
  blocking collectives  117 us (35%)
  local copies, waits for them, and re-layouts  69.7 us (21%)
  waiting for transfers between devices  60.2 us (18%)
  matrix products  34.4 us (10%)
  starting transfers between devices  25.9 us (8%)
  between operations  15.3 us (5%)
  other arithmetic  7.11 us (2%)
    all_to_all x1, blocking collectives, per_device(): lax.all_to_all(send_rows, ('sp', 'tp'), split_axis=0, concat_axis=0, tile...  51.9 us
    scatter x1, local copies, waits for them, and re-layouts, per_device(): send_rows = jnp.zeros((expert_total, capacity, model_width), jnp.bfloat16...  46.2 us
    all_to_all x1, waiting for transfers between devices, per_device(): lax.all_to_all(finished, ('sp', 'tp'), split_axis=0, concat_axis=0, tiled...  45.9 us
    all_gather x1, blocking collectives, per_device(): value_piece_b = lax.all_gather(value_b, 'sp', axis=0, tiled=True)  32.8 us
    all_gather x1, blocking collectives, per_device(): value_piece_a = lax.all_gather(value_a, 'sp', axis=0, tiled=True)  32 us
    dot_general x2, matrix products, swiglu_rows(): return jnp.dot(hidden, w_down, preferred_element_type=jnp.float32)  13.8 us
    ppermute x3, starting transfers between devices, gather_around(): lax.ppermute(going_down, axis, [(d, (d - 1) % ways) for d in range(ways)])  12.5 us
    dot_general x4, matrix products, online_update(): jnp.einsum('qhd,khd->hqk', query_map, key_map, preferred_element_type=jnp...  9.31 us
  transfers between devices with their start and end apart: 11, of which 6 were waited for; matrix products, arithmetic and copies ran while one was open for 6% of the time, Pallas kernels for 0%

profile of v1, /device:TPU:0, one launch (start us, length us, event | category | flops | bytes accessed | tf_op | source)
XLA Modules:
  0.0 329.3 jit_solution(9653954770351036120)
XLA Ops:
  6.5 3.0 collective-permute-start
  9.6 3.1 collective-permute-start.1
  12.7 0.8 copy.41
  13.7 32.8 %all_gather.11 = bf16[2048,1,128]{2,0,1:T(8,128)(2,1)S(1)} all-gather(bf16[256,1,128]{2,0,1:T(8,128)(2,1)} %param.26), channel_id=1, replica_groups=mesh['sp'=8,'tp'=4] {'sp'}, dimensions={0}, use_global_device_ids=true | all-gather | bytes 589824 | tf_op jit(solution)/shard_map/all_gather | solution.py:126
  46.5 32.0 %all_gather.9 = bf16[2048,1,128]{2,0,1:T(8,128)(2,1)S(1)} all-gather(bf16[256,1,128]{2,0,1:T(8,128)(2,1)} %param.23), channel_id=1, replica_groups=mesh['sp'=8,'tp'=4] {'sp'}, dimensions={0}, use_global_device_ids=true | all-gather | bytes 589824 | tf_op jit(solution)/shard_map/all_gather | solution.py:124
  79.4 0.9 broadcast_in_dim.50
  80.3 0.6 constant_dynamic-update-slice_fusion.7
  82.7 4.7 %collective-permute-start.3 = (bf16[256,1,128]{2,0,1:T(8,128)(2,1)S(1)}, bf16[256,1,128]{2,0,1:T(8,128)(2,1)S(1)}, u32[]{:S(2)}, u32[]{:S(2)}) collective-permute-start(bf16[256,1,128]{2,0,1:T(8,128)(2,1)S(1)} %collective-permute-done.1), channel_id=1, source_target_pairs={{0,28},{4,0},{8,4},{12,8},{16,12},{20,16},{24,20},{28,24},{1,29},{... | collective-permute-start | bytes 196616 | tf_op jit(solution)/shard_map/ppermute | solution.py:22
  87.4 0.6 constant_dynamic-update-slice_fusion.6
  88.0 0.6 constant_dynamic-update-slice_fusion.5
  88.6 1.0 collective-permute-done.2
  89.6 4.7 %collective-permute-start.5 = (bf16[256,1,128]{2,0,1:T(8,128)(2,1)S(1)}, bf16[256,1,128]{2,0,1:T(8,128)(2,1)S(1)}, u32[]{:S(2)}, u32[]{:S(2)}) collective-permute-start(bf16[256,1,128]{2,0,1:T(8,128)(2,1)S(1)} %collective-permute-done.3), channel_id=1, source_target_pairs={{0,28},{4,0},{8,4},{12,8},{16,12},{20,16},{24,20},{28,24},{1,29},{... | collective-permute-start | bytes 196616 | tf_op jit(solution)/shard_map/ppermute | solution.py:22
  94.3 0.6 constant_dynamic-update-slice_fusion.4
  95.0 0.6 constant_dynamic-update-slice_fusion.3
  95.6 1.0 collective-permute-done.4
  96.6 0.6 constant_dynamic-update-slice_fusion.2
  97.2 0.6 constant_dynamic-update-slice_fusion.1
  97.8 5.7 %collective-permute-done.6 = bf16[256,1,128]{2,0,1:T(8,128)(2,1)S(1)} collective-permute-done((bf16[256,1,128]{2,0,1:T(8,128)(2,1)S(1)}, bf16[256,1,128]{2,0,1:T(8,128)(2,1)S(1)}, u32[]{:S(2)}, u32[]{:S(2)}) %collective-permute-start.6) | collective-permute-done | bytes 65568 | tf_op jit(solution)/shard_map/ppermute | solution.py:19
  103.5 0.6 constant_dynamic-update-slice_fusion
  104.2 2.9 fusion.97
  107.1 3.0 fusion.96
  110.1 1.7 fusion.99
  111.8 1.7 fusion.98
  113.6 1.5 fusion.21
  118.3 0.7 reduce.22
  119.1 0.7 reshape.432
  119.7 3.3 all-to-all-start.1
  123.1 0.7 reduce.23
  123.9 0.6 reshape.434
  124.5 2.6 all-to-all-done.1
  127.1 3.3 all-to-all-start
  130.6 3.9 %all-to-all-done = bf16[4,2,4096]{2,1,0:T(2,128)(2,1)S(1)} async-done(((bf16[4,2,4096]{2,1,0:T(2,128)(2,1)}), bf16[4,2,4096]{2,1,0:T(2,128)(2,1)S(1)}, u32[]{:S(2)}, u32[]{:S(2)}) %all-to-all-start) | async-done | bytes 65568 | tf_op jit(solution)/shard_map/all_to_all | solution.py:155
  134.7 3.2 multiply_reduce_fusion.1
  138.0 2.3 gather_fusion
  140.3 1.6 broadcast_in_dim.53
  142.0 46.2 %scatter_fusion = bf16[32,16,2048]{2,1,0:T(8,128)(2,1)} fusion(bf16[32,16,2048]{2,1,0:T(8,128)(2,1)} %broadcast_in_dim.53, s32[256]{0:T(256)S(1)} %bitcast.177, bf16[256,2048]{1,0:T(8,128)(2,1)} %gather_fusion), kind=kCustom, calls=%fused_computation.2 | custom fusion | bytes 3147776 | tf_op jit(solution)/shard_map/scatter | solution.py:184
  188.2 51.9 %all_to_all.40 = bf16[32,16,2048]{2,1,0:T(8,128)(2,1)S(1)} all-to-all(bf16[32,16,2048]{2,1,0:T(8,128)(2,1)} %scatter_fusion), channel_id=1, replica_groups=mesh['sp'=8,'tp'=4] {'sp','tp'}, dimensions={0} | all-to-all | bytes 4194304 | tf_op jit(solution)/shard_map/all_to_all | solution.py:186
  240.1 1.3 copy-done.3
  241.4 3.6 %fusion.4 = f32[512,1024]{1,0:T(8,128)} fusion(bf16[512,2048]{1,0:T(8,128)(2,1)S(1)} %bitcast.179, bf16[1,2048,1024]{2,1,0:T(8,128)(2,1)S(1)} %copy-done.9), kind=kOutput, calls=%fused_computation.7 | convolution fusion | flops 2147483648 | bytes 8388608 | tf_op jit(solution)/shard_map/dot_general | solution.py:30
  245.1 10.6 %fusion.6 = bf16[512,2048]{1,0:T(8,128)(2,1)} fusion(bf16[1,1024,2048]{2,1,0:T(8,128)(2,1)} %param.36, f32[512,1024]{1,0:T(8,128)} %fusion.4, bf16[512,2048]{1,0:T(8,128)(2,1)} %bitcast.180, bf16[1,2048,1024]{2,1,0:T(8,128)(2,1)} %param.35), kind=kOutput, calls=%fused_computation.9 | convolution fusion | flops 4299161600 | bytes 14680064 | tf_op jit(solution)/shard_map/dot_general | solution.py:33
  255.7 3.7 %all-to-all-start.3 = ((bf16[32,16,2048]{2,1,0:T(8,128)(2,1)}), bf16[32,16,2048]{2,1,0:T(8,128)(2,1)}, u32[]{:S(2)}, u32[]{:S(2)}) async-start(bf16[32,16,2048]{2,1,0:T(8,128)(2,1)} %bitcast.178), calls=%async_computation.3 | async-start | bytes 4194304 | tf_op jit(solution)/shard_map/all_to_all | solution.py:193
  259.4 0.7 copy.45
  260.1 2.1 fusion.100
  262.2 45.9 %all-to-all-done.3 = bf16[32,16,2048]{2,1,0:T(8,128)(2,1)} async-done(((bf16[32,16,2048]{2,1,0:T(8,128)(2,1)}), bf16[32,16,2048]{2,1,0:T(8,128)(2,1)}, u32[]{:S(2)}, u32[]{:S(2)}) %all-to-all-start.3) | async-done | bytes 2097184 | tf_op jit(solution)/shard_map/all_to_all | solution.py:193
  308.1 5.1 %gather_fusion.1 = bf16[256,2048]{1,0:T(8,128)(2,1)} fusion(bf16[32,16,2048]{2,1,0:T(8,128)(2,1)} %all-to-all-done.3, s32[256]{0:T(256)S(1)} %bitcast.176), kind=kCustom, calls=%fused_computation.1 | custom fusion | bytes 2099200 | tf_op jit(solution)/shard_map/gather | solution.py:194
  313.3 2.7 reshape.410
  316.0 3.2 multiply_reduce_fusion
  319.2 3.2 fusion.16
  (71 shorter events, 5.1 us)
Async XLA Ops:
  6.5 312.7 %copy-start = (bf16[512,2048]{1,0:T(8,128)(2,1)S(1)}, bf16[512,2048]{1,0:T(8,128)(2,1)}, u32[]{:S(2)}) copy-start(bf16[512,2048]{1,0:T(8,128)(2,1)} %param.39) | copy-start | bytes 6291460
  6.5 73.8 %copy-start.5 = (bf16[256,1,128]{2,0,1:T(8,128)(2,1)S(1)}, bf16[256,1,128]{2,0,1:T(8,128)(2,1)}, u32[]{:S(2)}) copy-start(bf16[256,1,128]{2,0,1:T(8,128)(2,1)} %param.22) | copy-start | bytes 196612
  6.5 97.6 %copy-start.11 = (bf16[256,1,128]{2,0,1:T(8,128)(2,1)S(1)}, bf16[256,1,128]{2,0,1:T(8,128)(2,1)}, u32[]{:S(2)}) copy-start(bf16[256,1,128]{2,0,1:T(8,128)(2,1)} %param.21) | copy-start | bytes 196612
  6.5 103.5 %all-gather.2.cloned.1.call-start = ((), (), s32[]{:S(2)}) async-start(), calls=%async_computation.4 | async-start | bytes 1179648 | tf_op jit(solution)/shard_map/all_gather | solution.py:125
  6.5 76.1 %collective-permute-start = (bf16[256,1,128]{2,0,1:T(8,128)(2,1)}, bf16[256,1,128]{2,0,1:T(8,128)(2,1)S(1)}, u32[]{:S(2)}, u32[]{:S(2)}) collective-permute-start(bf16[256,1,128]{2,0,1:T(8,128)(2,1)} %param.22), channel_id=1, source_target_pairs={{0,4},{4,8},{8,12},{12,16},{16,20},{20,24},{24,28},{28,0},{1,5},{5... | collective-permute-start | bytes 196616 | tf_op jit(solution)/shard_map/ppermute | solution.py:19
  9.6 73.1 %collective-permute-start.1 = (bf16[256,1,128]{2,0,1:T(8,128)(2,1)}, bf16[256,1,128]{2,0,1:T(8,128)(2,1)S(1)}, u32[]{:S(2)}, u32[]{:S(2)}) collective-permute-start(bf16[256,1,128]{2,0,1:T(8,128)(2,1)} %param.22), channel_id=1, source_target_pairs={{0,28},{4,0},{8,4},{12,8},{16,12},{20,16},{24,20},{28,24},{1,29},{... | collective-permute-start | bytes 196616 | tf_op jit(solution)/shard_map/ppermute | solution.py:22
  82.6 7.0 %collective-permute-start.2 = (bf16[256,1,128]{2,0,1:T(8,128)(2,1)S(1)}, bf16[256,1,128]{2,0,1:T(8,128)(2,1)S(1)}, u32[]{:S(2)}, u32[]{:S(2)}) collective-permute-start(bf16[256,1,128]{2,0,1:T(8,128)(2,1)S(1)} %collective-permute-done), channel_id=1, source_target_pairs={{0,4},{4,8},{8,12},{12,16},{16,20},{20,24},{24,28},{28,0},{1,5},{5... | collective-permute-start | bytes 196616 | tf_op jit(solution)/shard_map/ppermute | solution.py:19
  82.7 6.9 %collective-permute-start.3 = (bf16[256,1,128]{2,0,1:T(8,128)(2,1)S(1)}, bf16[256,1,128]{2,0,1:T(8,128)(2,1)S(1)}, u32[]{:S(2)}, u32[]{:S(2)}) collective-permute-start(bf16[256,1,128]{2,0,1:T(8,128)(2,1)S(1)} %collective-permute-done.1), channel_id=1, source_target_pairs={{0,28},{4,0},{8,4},{12,8},{16,12},{20,16},{24,20},{28,24},{1,29},{... | collective-permute-start | bytes 196616 | tf_op jit(solution)/shard_map/ppermute | solution.py:22
  89.6 7.0 %collective-permute-start.4 = (bf16[256,1,128]{2,0,1:T(8,128)(2,1)S(1)}, bf16[256,1,128]{2,0,1:T(8,128)(2,1)S(1)}, u32[]{:S(2)}, u32[]{:S(2)}) collective-permute-start(bf16[256,1,128]{2,0,1:T(8,128)(2,1)S(1)} %collective-permute-done.2), channel_id=1, source_target_pairs={{0,4},{4,8},{8,12},{12,16},{16,20},{20,24},{24,28},{28,0},{1,5},{5... | collective-permute-start | bytes 196616 | tf_op jit(solution)/shard_map/ppermute | solution.py:19
  89.6 7.6 %collective-permute-start.5 = (bf16[256,1,128]{2,0,1:T(8,128)(2,1)S(1)}, bf16[256,1,128]{2,0,1:T(8,128)(2,1)S(1)}, u32[]{:S(2)}, u32[]{:S(2)}) collective-permute-start(bf16[256,1,128]{2,0,1:T(8,128)(2,1)S(1)} %collective-permute-done.3), channel_id=1, source_target_pairs={{0,28},{4,0},{8,4},{12,8},{16,12},{20,16},{24,20},{28,24},{1,29},{... | collective-permute-start | bytes 196616 | tf_op jit(solution)/shard_map/ppermute | solution.py:22
  96.6 7.0 %collective-permute-start.6 = (bf16[256,1,128]{2,0,1:T(8,128)(2,1)S(1)}, bf16[256,1,128]{2,0,1:T(8,128)(2,1)S(1)}, u32[]{:S(2)}, u32[]{:S(2)}) collective-permute-start(bf16[256,1,128]{2,0,1:T(8,128)(2,1)S(1)} %collective-permute-done.4), channel_id=1, source_target_pairs={{0,4},{4,8},{8,12},{12,16},{16,20},{20,24},{24,28},{28,0},{1,5},{5... | collective-permute-start | bytes 196616 | tf_op jit(solution)/shard_map/ppermute | solution.py:19
  107.1 3.0 copy-start.10
  110.1 3.5 %copy-start.2 = (f32[256,2048]{0,1:T(8,128)S(1)}, f32[256,2048]{0,1:T(8,128)}, u32[]{:S(2)}) copy-start(f32[256,2048]{0,1:T(8,128)} %get-tuple-element.62) | copy-start | bytes 6291460
  111.8 1.8 copy-start.1
  116.9 0.7 copy-start.8
  117.5 17.1 %copy-start.4 = (bf16[64,2048]{1,0:T(8,128)(2,1)S(1)}, bf16[64,2048]{1,0:T(8,128)(2,1)}, u32[]{:S(2)}) copy-start(bf16[64,2048]{1,0:T(8,128)(2,1)} %param.20) | copy-start | bytes 786436
  119.7 7.4 %all-to-all-start.1 = ((bf16[4,2,4096]{2,1,0:T(2,128)(2,1)}), bf16[4,2,4096]{2,1,0:T(2,128)(2,1)S(1)}, u32[]{:S(2)}, u32[]{:S(2)}) async-start(bf16[4,2,4096]{2,1,0:T(2,128)(2,1)} %reshape.432), calls=%async_computation.1 | async-start | bytes 131072 | tf_op jit(solution)/shard_map/all_to_all | solution.py:156
  127.1 7.4 %all-to-all-start = ((bf16[4,2,4096]{2,1,0:T(2,128)(2,1)}), bf16[4,2,4096]{2,1,0:T(2,128)(2,1)S(1)}, u32[]{:S(2)}, u32[]{:S(2)}) async-start(bf16[4,2,4096]{2,1,0:T(2,128)(2,1)} %reshape.434), calls=%async_computation | async-start | bytes 131072 | tf_op jit(solution)/shard_map/all_to_all | solution.py:155
  134.7 3.2 copy-start.6
  188.2 53.2 %copy-start.9 = (bf16[1,2048,1024]{2,1,0:T(8,128)(2,1)S(1)}, bf16[1,2048,1024]{2,1,0:T(8,128)(2,1)}, u32[]{:S(2)}) copy-start(bf16[1,2048,1024]{2,1,0:T(8,128)(2,1)} %param.34) | copy-start | bytes 12582916
  240.1 1.3 copy-start.3
  255.7 3.7 %copy-start.7 = (f32[64,4]{0,1:T(4,128)S(1)}, f32[64,4]{0,1:T(4,128)}, u32[]{:S(2)}) copy-start(f32[64,4]{0,1:T(4,128)} %param.33) | copy-start | bytes 3076
  255.7 52.4 %all-to-all-start.3 = ((bf16[32,16,2048]{2,1,0:T(8,128)(2,1)}), bf16[32,16,2048]{2,1,0:T(8,128)(2,1)}, u32[]{:S(2)}, u32[]{:S(2)}) async-start(bf16[32,16,2048]{2,1,0:T(8,128)(2,1)} %bitcast.178), calls=%async_computation.3 | async-start | bytes 4194304 | tf_op jit(solution)/shard_map/all_to_all | solution.py:193
Sparse Core Ops, SparseCore 0:
  12.8 42.1 all-gather.1
